TPU v7x, 32 devices: a whole 2x2x4 slice. The times are simulated.
32 devices in a mesh: grp: 2 (over y), sp: 4 (over z), tp: 4 (over x, core).
Axes of the slice: x: 2, y: 2, z: 4, core: 2. Of those that a mesh axis runs over, the one named last changes fastest.
Arguments:
- hidden: bfloat16 [3072, 2048], P(('grp', 'sp'), 'tp'), parts along dimension 0, may hold values from -45 to 45
- norm_gain: bfloat16 [2048], replicated, may hold values from 0.099609375 to 1.8984375
- w_query: bfloat16 [2048, 1024], P(None, 'tp'), may hold values from -0.125 to 0.125
- w_key: bfloat16 [2048, 1024], P(None, 'tp'), may hold values from -0.125 to 0.125
- w_value: bfloat16 [2048, 1024], P(None, 'tp'), may hold values from -0.125 to 0.125
- query_gain: float32 [8, 128], P('tp'), may hold values from 0.3 to 16
- key_gain: float32 [8, 128], P('tp'), may hold values from 0.3 to 16
- w_out: bfloat16 [1024, 2048], P('tp'), may hold values from -1.5 to 1.5
Outputs:
- mixed: bfloat16 [3072, 2048], P(('grp', 'sp'), 'tp'), parts along dimension 0
- log_total: float32 [3072, 8], P(('grp', 'sp'), 'tp'), parts along dimension 0
There are 2 independent parts, one for each index of `grp`. A program takes and returns all parts, laid end to end along the dimension named above; an argument that names none is the same for every part. Nothing has to cross between parts.
All inputs are finite; a program needn't handle non-finite values.
Results may differ from a plain program's by a relative error of at most 0.015.
The roundings to bfloat16 on the way count: a program that leaves them out, or rounds other values in their place, can miss the bound.
Values may be sent and summed in bfloat16 or wider, within the bound.
No kernel may reach another device: no remote copies, remote signals or barrier semaphores. Data moves between devices by JAX's collectives and lax.ppermute only.
A program may use at most 64 MiB of HBM per device.

v0:
```python
import math
import jax
import jax.numpy as jnp
from jax import lax
from jax.sharding import PartitionSpec as P

D = 2048
KEYS_BEHIND = 128
MIDDLE_DILATION = 4
WIDEST_DILATION = 16
EPSILON = 1e-06
ROTARY_BASE = 500000.0


def from_behind(value, axis, steps):
    count = lax.axis_size(axis)
    initial, last = (max(0, -steps), min(count, count - steps))
    return lax.ppermute(value, axis, [(source, source + steps) for source in range(initial, last)])


def rotate(values, positions):
    head_width = values.shape[-1]
    inverse = ROTARY_BASE ** (-jnp.arange(0, head_width, 2, dtype=jnp.float32) / head_width)
    angles = positions[:, None] * inverse[None, :]
    cosine = jnp.cos(angles)[:, None, :]
    sine = jnp.sin(angles)[:, None, :]
    half_width = head_width // 2
    first_half = values[..., :half_width]
    second_half = values[..., half_width:]
    return jnp.concatenate(
        [first_half * cosine - second_half * sine, second_half * cosine + first_half * sine],
        axis=-1,
    )


def head_norm(values, gains):
    normed = values * lax.rsqrt(jnp.mean(values * values, axis=-1, keepdims=True) + EPSILON)
    return normed * gains[None, :, :]


def earlier_pairs(own_pair, token_rows):
    distant_shards = (KEYS_BEHIND * WIDEST_DILATION + token_rows - 1) // token_rows
    pieces = [own_pair]
    for distance in range(1, distant_shards + 1):
        pieces.insert(0, from_behind(own_pair, "sp", distance))
    buffer = jnp.concatenate(pieces, axis=1)
    return buffer


def local_branch(query, key_rows, value_rows, dilation_step, first_pos):
    token_rows, head_count, head_width = query.shape
    reach_rows = KEYS_BEHIND * dilation_step
    buffer_rows = key_rows.shape[0]
    class_rows = token_rows // dilation_step
    class_keys = class_rows + KEYS_BEHIND
    window_start = buffer_rows - token_rows - reach_rows
    key_window = key_rows[window_start:]
    value_window = value_rows[window_start:]
    query_class = query.reshape(class_rows, dilation_step, head_count, head_width).transpose(
        1, 0, 2, 3
    )
    key_class = key_window.reshape(class_keys, dilation_step, head_count, head_width).transpose(
        1, 0, 2, 3
    )
    value_class = value_window.reshape(class_keys, dilation_step, head_count, head_width).transpose(
        1, 0, 2, 3
    )
    block_rows = math.gcd(class_rows, KEYS_BEHIND) if class_rows > KEYS_BEHIND else class_rows
    block_count = class_rows // block_rows
    query_blocks = query_class.reshape(
        dilation_step, block_count, block_rows, head_count, head_width
    )
    key_blocks = jnp.stack(
        [
            key_class[:, number * block_rows : number * block_rows + block_rows + KEYS_BEHIND]
            for number in range(block_count)
        ],
        axis=1,
    )
    value_blocks = jnp.stack(
        [
            value_class[:, number * block_rows : number * block_rows + block_rows + KEYS_BEHIND]
            for number in range(block_count)
        ],
        axis=1,
    )
    scores = jnp.einsum(
        "rnqhd,rnkhd->rnhqk", query_blocks, key_blocks, preferred_element_type=jnp.float32
    ) * head_width ** (-0.5)
    row_index = jnp.arange(block_rows, dtype=jnp.int32)[:, None]
    col_index = jnp.arange(block_rows + KEYS_BEHIND, dtype=jnp.int32)[None, :]
    distance = KEYS_BEHIND + row_index - col_index
    in_band = (distance >= 0) & (distance <= KEYS_BEHIND)
    class_index = jnp.arange(block_count, dtype=jnp.int32)[:, None] * block_rows + col_index
    residue = jnp.arange(dilation_step, dtype=jnp.int32)[:, None, None]
    key_position = first_pos - reach_rows + class_index[None] * dilation_step + residue
    allowed = in_band[None, None, None, :, :] & (key_position >= 0)[:, :, None, None, :]
    scores = jnp.where(allowed, scores, -jnp.inf)
    row_max = jnp.max(scores, axis=-1, keepdims=True)
    weights = jnp.exp(scores - row_max)
    weight_sum = jnp.sum(weights, axis=-1)
    weighted = jnp.einsum(
        "rnhqk,rnkhd->rnqhd",
        weights.astype(jnp.bfloat16),
        value_blocks,
        preferred_element_type=jnp.float32,
    )
    branch_out = weighted / jnp.transpose(weight_sum, (0, 1, 3, 2))[..., None]
    branch_out = branch_out.reshape(dilation_step, class_rows, head_count, head_width).transpose(
        1, 0, 2, 3
    )
    branch_out = branch_out.reshape(token_rows, head_count, head_width)
    log_sum = jnp.transpose(row_max[..., 0] + jnp.log(weight_sum), (0, 1, 3, 2))
    log_sum = (
        log_sum.reshape(dilation_step, class_rows, head_count)
        .transpose(1, 0, 2)
        .reshape(token_rows, head_count)
    )
    return (branch_out, log_sum)


def local(hidden, norm_gain, w_query, w_key, w_value, query_gain, key_gain, w_out):
    token_rows = hidden.shape[0]
    local_width = w_query.shape[1]
    head_count = query_gain.shape[0]
    head_width = query_gain.shape[1]
    gain_full = norm_gain.astype(jnp.float32)
    raw_piece = lax.all_gather(hidden, "tp", axis=1, tiled=True).astype(jnp.float32)
    scaled = (raw_piece * gain_full[None, :]).astype(jnp.bfloat16)

    def add_product(weight):
        return jnp.dot(scaled, weight, preferred_element_type=jnp.float32)

    query_raw = add_product(w_query)
    key_raw = add_product(w_key)
    value_raw = add_product(w_value)
    squares = jnp.sum(raw_piece * raw_piece, axis=1)
    row_scale = lax.rsqrt(squares / D + EPSILON)[:, None]
    first_pos = lax.axis_index("sp") * token_rows
    positions = (jnp.arange(token_rows, dtype=jnp.int32) + first_pos).astype(jnp.float32)
    query = rotate(
        head_norm((query_raw * row_scale).reshape(token_rows, head_count, head_width), query_gain),
        positions,
    ).astype(jnp.bfloat16)
    key_now = rotate(
        head_norm((key_raw * row_scale).reshape(token_rows, head_count, head_width), key_gain),
        positions,
    ).astype(jnp.bfloat16)
    value_now = (value_raw * row_scale).astype(jnp.bfloat16)
    own_pair = jnp.stack([key_now.reshape(token_rows, local_width), value_now], axis=0)
    buffer = earlier_pairs(own_pair, token_rows)
    key_rows = buffer[0].reshape(-1, head_count, head_width)
    value_rows = buffer[1].reshape(-1, head_count, head_width)
    branch_outs = []
    branch_logs = []
    for dilation_step in (1, MIDDLE_DILATION, WIDEST_DILATION):
        branch_out, log_sum = local_branch(query, key_rows, value_rows, dilation_step, first_pos)
        branch_outs.append(branch_out)
        branch_logs.append(log_sum)
    stacked_logs = jnp.stack(branch_logs, axis=0)
    peak = jnp.max(stacked_logs, axis=0)
    log_total = peak + jnp.log(jnp.sum(jnp.exp(stacked_logs - peak[None]), axis=0))
    shares = jnp.exp(stacked_logs - log_total[None])
    attended = jnp.sum(shares[..., None] * jnp.stack(branch_outs, axis=0), axis=0)
    attended = attended.astype(jnp.bfloat16).reshape(token_rows, local_width)
    column_block = lax.all_to_all(w_out, "tp", split_axis=1, concat_axis=0, tiled=True)
    mixed = jnp.dot(
        lax.all_gather(attended, "tp", axis=1, tiled=True),
        column_block,
        preferred_element_type=jnp.float32,
    )
    return (mixed.astype(jnp.bfloat16), log_total)


def solution(mesh):
    placed = (
        P(("grp", "sp"), "tp"),
        P(),
        P(None, "tp"),
        P(None, "tp"),
        P(None, "tp"),
        P("tp", None),
        P("tp", None),
        P("tp", None),
    )
    return jax.shard_map(
        local,
        mesh=mesh,
        in_specs=placed,
        out_specs=(P(("grp", "sp"), "tp"), P(("grp", "sp"), "tp")),
        check_vma=False,
    )
```

profile of v0, /device:TPU:17, one launch (start us, length us, event | category | flops | bytes accessed | tf_op | source)
XLA Modules:
  0.0 135.2 jit_solution(7337849643305904054)
XLA Ops:
  7.2 0.7 all-gather.2.cloned.1.call-update
  7.9 2.3 %copy.167 = bf16[256,2048]{0,1:T(8,128)(2,1)} copy(bf16[256,2048]{1,0:T(8,128)(2,1)} %param.15) | data formatting | bytes 2097152 | tf_op args[7]
  10.2 4.3 %all-to-all-start = ((bf16[256,4,512]{0,2,1:T(8,128)(2,1)}), bf16[256,4,512]{0,2,1:T(8,128)(2,1)S(1)}, u32[]{:S(2)}, u32[]{:S(2)}) async-start(bf16[256,4,512]{0,2,1:T(8,128)(2,1)} %bitcast.65), calls=%async_computation | async-start | bytes 2097152 | tf_op jit(solution)/shard_map/all_to_all | solution.py:166
  15.0 0.7 broadcast_and_fusion.1
  15.6 0.7 broadcast_and_fusion.2
  16.3 1.4 %multiply_cosine_fusion = (f32[384,64]{1,0:T(8,128)S(1)}, f32[384,64]{1,0:T(8,128)}) fusion(f32[64]{0:T(128)S(1)} %multiply_power_fusion, f32[384]{0:T(512)S(1)} %add_convert_fusion.2), kind=kLoop, calls=%fused_computation.71 | loop fusion | flops 24576 | bytes 198400 | tf_op jit(solution)/shard_map/cos | solution.py:25
  17.8 20.8 %all-gather.2.cloned.1.call-done = bf16[384,2048]{1,0:T(8,128)(2,1)} async-done(((bf16[384,512]{1,0:T(8,128)(2,1)}), bf16[384,2048]{1,0:T(8,128)(2,1)}) %all-gather.2.cloned.1.call-update) | async-done | bytes 1572880 | tf_op jit(solution)/shard_map/all_gather | solution.py:128
  38.6 1.9 %fusion.1 = f32[384]{0:T(512)S(1)} fusion(bf16[384,2048]{1,0:T(8,128)(2,1)} %all-gather.2.cloned.1.call-done), kind=kLoop, calls=%fused_computation.3 | loop fusion | flops 2358912 | bytes 1574400 | tf_op jit(solution)/shard_map/reduce_sum | solution.py:137
  40.5 0.8 multiply_reduce_fusion
  41.5 2.5 %multiply_reduce_fusion.1 = (f32[384,2]{0,1:T(2,128)S(1)}, f32[384,256]{0,1:T(8,128)S(1)}) fusion(f32[384]{0:T(512)S(1)} %add_rsqrt_fusion.2, bf16[2048,256]{1,0:T(8,128)(2,1)} %param.10, bf16[384,2048]{1,0:T(8,128)(2,1)} %all-gather.2.cloned.1.call-done, f32[2048]{0:T(1024)S(1)} %convert_element_type.58), kind=kOutput, calls=%fused_computation.69 | convolution fusion | flops 405306624 | bytes 3027456 | tf_op jit(solution)/shard_map/dot_general | solution.py:132
  44.4 1.3 subtract_convert_fusion.1
  46.0 2.5 %fusion.20 = bf16[1,384,256]{1,2,0:T(8,128)(2,1)S(1)} fusion(bf16[2048,256]{1,0:T(8,128)(2,1)} %param.12, bf16[384,2048]{1,0:T(8,128)(2,1)} %all-gather.2.cloned.1.call-done, f32[2048]{0:T(1024)S(1)} %convert_element_type.58, f32[384]{0:T(512)S(1)} %add_rsqrt_fusion.2), kind=kOutput, calls=%fused_computation.25 | convolution fusion | flops 405209088 | bytes 2827776 | tf_op jit(solution)/shard_map/dot_general | solution.py:132
  48.6 0.8 pad_maximum_fusion.2
  49.4 0.7 collective-permute-start.2
  50.1 1.4 %collective-permute-start.3 = (bf16[2,384,256]{1,2,0:T(8,128)(2,1)}, bf16[2,384,256]{1,2,0:T(8,128)(2,1)}, u32[]{:S(2)}, u32[]{:S(2)}) collective-permute-start(bf16[2,384,256]{1,2,0:T(8,128)(2,1)} %pad_maximum_fusion.2), channel_id=1, source_target_pairs={{0,12},{1,13},{2,14},{3,15},{16,28},{17,29},{18,30},{19,31}} | collective-permute-start | bytes 1179656 | tf_op jit(solution)/shard_map/ppermute | solution.py:18
  51.5 0.7 broadcast_and_fusion
  52.2 1.3 copy.168
  53.5 1.3 collective-permute-start.1
  54.8 3.3 %collective-permute-start = (bf16[2,384,256]{1,2,0:T(8,128)(2,1)}, bf16[2,384,256]{1,2,0:T(8,128)(2,1)S(1)}, u32[]{:S(2)}, u32[]{:S(2)}) collective-permute-start(bf16[2,384,256]{1,2,0:T(8,128)(2,1)} %pad_maximum_fusion.2), channel_id=1, source_target_pairs={{0,4},{4,8},{8,12},{1,5},{5,9},{9,13},{2,6},{6,10},{10,14},{3,7},{... | collective-permute-start | bytes 1179656 | tf_op jit(solution)/shard_map/ppermute | solution.py:18
  58.0 0.7 copy.150
  58.8 0.7 copy.149
  59.5 0.7 copy.145
  60.2 0.7 copy.144
  61.1 1.1 constant_dynamic-update-slice_fusion.3
  62.2 10.8 %collective-permute-done.1 = bf16[2,384,256]{1,2,0:T(8,128)(2,1)S(1)} collective-permute-done((bf16[2,384,256]{1,2,0:T(8,128)(2,1)}, bf16[2,384,256]{1,2,0:T(8,128)(2,1)S(1)}, u32[]{:S(2)}, u32[]{:S(2)}) %collective-permute-start.1) | collective-permute-done | bytes 393248 | tf_op jit(solution)/shard_map/ppermute | solution.py:18
  73.0 17.4 %collective-permute-done = bf16[2,384,256]{1,2,0:T(8,128)(2,1)S(1)} collective-permute-done((bf16[2,384,256]{1,2,0:T(8,128)(2,1)}, bf16[2,384,256]{1,2,0:T(8,128)(2,1)S(1)}, u32[]{:S(2)}, u32[]{:S(2)}) %collective-permute-start) | collective-permute-done | bytes 393248 | tf_op jit(solution)/shard_map/ppermute | solution.py:18
  90.6 0.6 copy-done.3
  91.5 1.5 %copy.151 = bf16[1,2432,256]{2,1,0:T(8,128)(2,1)} copy(bf16[1,2432,256]{1,2,0:T(8,128)(2,1)S(1)} %get-tuple-element.2) | data formatting | bytes 2490368 | tf_op jit(solution)/shard_map/slice | solution.py:57
  92.9 2.9 %reshape.537 = bf16[152,16,2,128]{3,2,1,0:T(2,128)(2,1)S(1)} reshape(bf16[1,2432,256]{2,1,0:T(8,128)(2,1)} %copy.151) | data formatting | bytes 2490368 | tf_op jit(solution)/shard_map/reshape | solution.py:62
  95.8 2.0 %fusion.85 = (f32[16,2,24]{2,1,0:T(2,128)S(1)}, f32[16,2,24,152]{3,2,1,0:T(8,128)S(1)}) fusion(bf16[152,16,2,128]{3,2,1,0:T(2,128)(2,1)S(1)} %reshape.537, bf16[24,16,2,64]{3,0,2,1:T(8,128)(2,1)} %copy.150, bf16[24,16,2,64]{3,0,2,1:T(8,128)(2,1)} %copy.149, pred[16,24,152]{2,1,0:T(8,128)(4,1)} %broadcast_and_fusion), kind=kOutput, calls=%fused_computation.142 | convolution fusion | flops 30627072 | bytes 1970176 | tf_op jit(solution)/shard_map/rnqhd,rnkhd->rnhqk/dot_general | solution.py:87
  97.8 0.9 copy-done.5
  99.1 0.6 copy-done.21
  99.7 0.7 stack_reshape.14
  100.4 0.7 stack.54
  101.1 2.1 %maximum_maximum_fusion = (bf16[1,896,256]{1,2,0:T(8,128)(2,1)S(1)}, bf16[1,896,256]{1,2,0:T(8,128)(2,1)}) fusion(bf16[1,384,256]{1,2,0:T(8,128)(2,1)} %copy-done.7, bf16[1,384,256]{1,2,0:T(8,128)(2,1)} %bitcast.176, bf16[2,384,256]{1,2,0:T(8,128)(2,1)} %copy-done.3, bf16[2,384,256]{1,2,0:T(8,128)(2,1)} %copy-done.15), kind=kLoop, calls=%fused_computation.43 | loop fusion | flops 3670016 | bytes 2097152 | tf_op jit(solution)/shard_map/slice | solution.py:57
  103.5 1.5 %fusion.86 = (f32[4,2,96]{2,1,0:T(2,128)S(1)}, f32[4,2,96,224]{3,2,1,0:T(8,128)S(1)}) fusion(bf16[224,4,2,128]{3,2,1,0:T(2,128)(2,1)S(1)} %reshape.535, bf16[96,4,2,64]{3,0,2,1:T(8,128)(2,1)S(1)} %copy-done.18, bf16[96,4,2,64]{3,0,2,1:T(8,128)(2,1)} %copy.144, pred[4,96,224]{2,1,0:T(8,128)(4,1)S(1)} %copy-done.20), kind=kOutput, calls=%fused_computation.143 | convolution fusion | flops 44948736 | bytes 1432576 | tf_op jit(solution)/shard_map/rnqhd,rnkhd->rnhqk/dot_general | solution.py:87
  105.4 0.5 copy-done.16
  106.1 0.7 stack_reshape.13
  106.8 0.7 stack.53
  107.5 0.8 copy.163
  108.3 1.2 reshape.542
  109.5 2.1 %fusion.29 = f32[24,16,2,128]{3,0,2,1:T(8,128)S(1)} fusion(bf16[152,16,2,128]{3,2,1,0:T(2,128)(2,1)} %reshape.542, f32[16,2,24,152]{3,2,1,0:T(8,128)S(1)} %copy-done.6, f32[16,2,24]{2,1,0:T(2,128)S(1)} %get-tuple-element.26, f32[16,24,2]{1,2,0:T(2,128)} %bitcast.200), kind=kOutput, calls=%fused_computation.30 | convolution fusion | flops 30216192 | bytes 2111488 | tf_op jit(solution)/shard_map/rnhqk,rnkhd->rnqhd/dot_general | solution.py:102
  112.1 0.6 copy-done.17
  115.0 0.4 fusion.87
  115.8 0.6 fusion.25
  116.6 0.4 fusion.16
  117.1 8.7 %all_gather.7 = bf16[384,1024]{0,1:T(8,128)(2,1)S(1)} all-gather(bf16[384,256]{0,1:T(8,128)(2,1)S(1)} %bitcast.191), channel_id=1, replica_groups=mesh['grp'=2,'sp'=4,'tp'=4] {'tp'}, dimensions={1}, use_global_device_ids=true | all-gather | bytes 983040 | tf_op jit(solution)/shard_map/all_gather | solution.py:168
  125.8 2.6 %convolution_convert_fusion = bf16[384,512]{1,0:T(8,128)(2,1)} fusion(bf16[384,1024]{0,1:T(8,128)(2,1)S(1)} %all_gather.7, bf16[1024,512]{1,0:T(8,128)(2,1)} %bitcast.190), kind=kOutput, calls=%fused_computation.10 | convolution fusion | flops 402849792 | bytes 2228224 | tf_op jit(solution)/shard_map/dot_general | solution.py:167
  (127 shorter events, 6.6 us)
Async XLA Ops:
  7.2 33.3 %copy-start = (bf16[2048,256]{1,0:T(8,128)(2,1)S(1)}, bf16[2048,256]{1,0:T(8,128)(2,1)}, u32[]{:S(2)}) copy-start(bf16[2048,256]{1,0:T(8,128)(2,1)} %param.11) | copy-start | bytes 3145732
  7.2 31.4 %all-gather.2.cloned.1.call-start = ((), (), s32[]{:S(2)}) async-start(), calls=%async_computation.1 | async-start | bytes 1966080 | tf_op jit(solution)/shard_map/all_gather | solution.py:128
  10.2 4.3 %copy-start.31 = (bf16[2048]{0:T(1024)(128)(2,1)S(1)}, bf16[2048]{0:T(1024)(128)(2,1)}, u32[]{:S(2)}) copy-start(bf16[2048]{0:T(1024)(128)(2,1)} %param.9) | copy-start | bytes 12292
  10.2 42.0 %all-to-all-start = ((bf16[256,4,512]{0,2,1:T(8,128)(2,1)}), bf16[256,4,512]{0,2,1:T(8,128)(2,1)S(1)}, u32[]{:S(2)}, u32[]{:S(2)}) async-start(bf16[256,4,512]{0,2,1:T(8,128)(2,1)} %bitcast.65), calls=%async_computation | async-start | bytes 2097152 | tf_op jit(solution)/shard_map/all_to_all | solution.py:166
  38.5 1.9 %copy-start.14 = (bf16[384,2048]{1,0:T(8,128)(2,1)S(1)}, bf16[384,2048]{1,0:T(8,128)(2,1)}, u32[]{:S(2)}) copy-start(bf16[384,2048]{1,0:T(8,128)(2,1)} %all-gather.2.cloned.1.call-done) | copy-start | bytes 4718596
  41.5 2.7 %copy-start.32 = (f32[2,128]{1,0:T(2,128)S(1)}, f32[2,128]{1,0:T(2,128)}, u32[]{:S(2)}) copy-start(f32[2,128]{1,0:T(2,128)} %param.14) | copy-start | bytes 3076
  41.5 2.7 %copy-start.33 = (f32[2,128]{1,0:T(2,128)S(1)}, f32[2,128]{1,0:T(2,128)}, u32[]{:S(2)}) copy-start(f32[2,128]{1,0:T(2,128)} %param.13) | copy-start | bytes 3076
  45.7 13.8 %copy-start.12 = (bf16[384,2,64]{2,0,1:T(8,128)(2,1)}, bf16[384,2,64]{2,0,1:T(8,128)(2,1)S(1)}, u32[]{:S(2)}) copy-start(bf16[384,2,64]{2,0,1:T(8,128)(2,1)S(1)} %get-tuple-element.9) | copy-start | bytes 294916
  45.7 14.5 %copy-start.10 = (bf16[384,2,64]{2,0,1:T(8,128)(2,1)}, bf16[384,2,64]{2,0,1:T(8,128)(2,1)S(1)}, u32[]{:S(2)}) copy-start(bf16[384,2,64]{2,0,1:T(8,128)(2,1)S(1)} %get-tuple-element.8) | copy-start | bytes 294916
  46.0 44.5 %copy-start.1 = (bf16[384,2,128]{0,2,1:T(8,128)(2,1)}, bf16[384,2,128]{0,2,1:T(8,128)(2,1)S(1)}, u32[]{:S(2)}) copy-start(bf16[384,2,128]{0,2,1:T(8,128)(2,1)S(1)} %copy.139) | copy-start | bytes 589828
  48.6 42.0 %copy-start.7 = (bf16[1,384,256]{1,2,0:T(8,128)(2,1)}, bf16[1,384,256]{1,2,0:T(8,128)(2,1)S(1)}, u32[]{:S(2)}) copy-start(bf16[1,384,256]{1,2,0:T(8,128)(2,1)S(1)} %fusion.20) | copy-start | bytes 589828
  49.4 11.5 %collective-permute-start.2 = (bf16[2,384,256]{1,2,0:T(8,128)(2,1)}, bf16[2,384,256]{1,2,0:T(8,128)(2,1)S(1)}, u32[]{:S(2)}, u32[]{:S(2)}) collective-permute-start(bf16[2,384,256]{1,2,0:T(8,128)(2,1)} %pad_maximum_fusion.2), channel_id=1, source_target_pairs={} | collective-permute-start | bytes 1179656 | tf_op jit(solution)/shard_map/ppermute | solution.py:18
  50.1 11.0 %collective-permute-start.3 = (bf16[2,384,256]{1,2,0:T(8,128)(2,1)}, bf16[2,384,256]{1,2,0:T(8,128)(2,1)}, u32[]{:S(2)}, u32[]{:S(2)}) collective-permute-start(bf16[2,384,256]{1,2,0:T(8,128)(2,1)} %pad_maximum_fusion.2), channel_id=1, source_target_pairs={{0,12},{1,13},{2,14},{3,15},{16,28},{17,29},{18,30},{19,31}} | collective-permute-start | bytes 1179656 | tf_op jit(solution)/shard_map/ppermute | solution.py:18
  53.5 19.5 %collective-permute-start.1 = (bf16[2,384,256]{1,2,0:T(8,128)(2,1)}, bf16[2,384,256]{1,2,0:T(8,128)(2,1)S(1)}, u32[]{:S(2)}, u32[]{:S(2)}) collective-permute-start(bf16[2,384,256]{1,2,0:T(8,128)(2,1)} %pad_maximum_fusion.2), channel_id=1, source_target_pairs={{0,8},{4,12},{1,9},{5,13},{2,10},{6,14},{3,11},{7,15},{16,24},{20,... | collective-permute-start | bytes 1179656 | tf_op jit(solution)/shard_map/ppermute | solution.py:18
  54.8 35.7 %collective-permute-start = (bf16[2,384,256]{1,2,0:T(8,128)(2,1)}, bf16[2,384,256]{1,2,0:T(8,128)(2,1)S(1)}, u32[]{:S(2)}, u32[]{:S(2)}) collective-permute-start(bf16[2,384,256]{1,2,0:T(8,128)(2,1)} %pad_maximum_fusion.2), channel_id=1, source_target_pairs={{0,4},{4,8},{8,12},{1,5},{5,9},{9,13},{2,6},{6,10},{10,14},{3,7},{... | collective-permute-start | bytes 1179656 | tf_op jit(solution)/shard_map/ppermute | solution.py:18
  73.0 17.6 %copy-start.15 = (bf16[2,384,256]{1,2,0:T(8,128)(2,1)}, bf16[2,384,256]{1,2,0:T(8,128)(2,1)S(1)}, u32[]{:S(2)}) copy-start(bf16[2,384,256]{1,2,0:T(8,128)(2,1)S(1)} %collective-permute-done.1) | copy-start | bytes 1179652
  90.5 0.7 copy-start.3
  97.8 0.9 copy-start.5
  99.0 0.6 copy-start.21
  101.1 2.5 %copy-start.18 = (bf16[96,4,2,64]{3,0,2,1:T(8,128)(2,1)S(1)}, bf16[96,4,2,64]{3,0,2,1:T(8,128)(2,1)}, u32[]{:S(2)}) copy-start(bf16[96,4,2,64]{3,0,2,1:T(8,128)(2,1)} %copy.145) | copy-start | bytes 294916
  101.1 2.5 %copy-start.20 = (pred[4,96,224]{2,1,0:T(8,128)(4,1)S(1)}, pred[4,96,224]{2,1,0:T(8,128)(4,1)}, u32[]{:S(2)}) copy-start(pred[4,96,224]{2,1,0:T(8,128)(4,1)} %broadcast_and_fusion.1) | copy-start | bytes 258052
  105.0 0.9 copy-start.16
  105.0 2.5 %copy-start.24 = (f32[4,2,96]{2,1,0:T(2,128)}, f32[4,2,96]{2,1,0:T(2,128)S(1)}, u32[]{:S(2)}) copy-start(f32[4,2,96]{2,1,0:T(2,128)S(1)} %get-tuple-element.28) | copy-start | bytes 9220
  105.9 1.6 %copy-start.26 = (f32[4,2,96]{2,1,0:T(2,128)}, f32[4,2,96]{2,1,0:T(2,128)S(1)}, u32[]{:S(2)}) copy-start(f32[4,2,96]{2,1,0:T(2,128)S(1)} %fusion.35) | copy-start | bytes 9220
  108.2 1.3 copy-start.6
  109.5 2.2 %copy-start.9 = (bf16[1,896,256]{1,2,0:T(8,128)(2,1)S(1)}, bf16[1,896,256]{1,2,0:T(8,128)(2,1)}, u32[]{:S(2)}) copy-start(bf16[1,896,256]{1,2,0:T(8,128)(2,1)} %get-tuple-element.5) | copy-start | bytes 1376260
  111.6 1.1 copy-start.17
  111.6 1.1 copy-start.25
  111.6 1.1 copy-start.27
  112.7 0.9 copy-start.2
  112.7 1.1 copy-start.4
  112.7 1.1 copy-start.8
  113.9 0.9 copy-start.11
  113.9 1.0 copy-start.13
  113.9 1.1 copy-start.19
  115.8 0.7 copy-start.28
  115.8 0.7 copy-start.29
  115.8 0.7 copy-start.22
  115.8 0.7 copy-start.23
  116.5 11.9 %copy-start.30 = (f32[384,2]{0,1:T(2,128)}, f32[384,2]{0,1:T(2,128)S(1)}, u32[]{:S(2)}) copy-start(f32[384,2]{0,1:T(2,128)S(1)} %log_add_fusion) | copy-start | bytes 9220
Sparse Core Ops, SparseCore 0:
  9.5 28.9 all-gather.1
where the time goes:
time: 136 us; the launch traced here: 135 us
  waiting for transfers between devices  49.7 us (37%)
  local copies, waits for them, and re-layouts  23.9 us (18%)
  matrix products  15.2 us (11%)
  between operations  14.8 us (11%)
  other arithmetic  12 us (9%)
  starting transfers between devices  11 us (8%)
  blocking collectives  8.71 us (6%)
    ppermute x4, waiting for transfers between devices, from_behind(): lax.ppermute(value, axis, [(source, source + steps) for source in range(i...  28.2 us
    all_gather x1, waiting for transfers between devices, local(): lax.all_gather(hidden, 'tp', axis=1, tiled=True).astype(jnp.float32)  20.8 us
    all_gather x1, blocking collectives, local(): lax.all_gather(attended, 'tp', axis=1, tiled=True)  8.71 us
    unnamed x81, local copies, waits for them, and re-layouts  8.5 us
    ppermute x4, starting transfers between devices, from_behind(): lax.ppermute(value, axis, [(source, source + steps) for source in range(i...  6.63 us
    dot_general x3, matrix products, add_product(): return jnp.dot(scaled, weight, preferred_element_type=jnp.float32)  5.79 us
    all_to_all x1, starting transfers between devices, local(): lax.all_to_all(w_out, 'tp', split_axis=1, concat_axis=0, tiled=True)  4.29 us
    dot_general x3, matrix products, local_branch(): jnp.einsum('rnqhd,rnkhd->rnhqk', query_blocks, key_blocks, preferred_elem...  3.85 us
  transfers between devices with their start and end apart: 6, of which 3 were waited for; matrix products, arithmetic and copies ran while one was open for 16% of the time, Pallas kernels for 0%

commit v1 on v0

--- a/solution.py
+++ b/solution.py
@@ -125,7 +125,7 @@
     head_count = query_gain.shape[0]
     head_width = query_gain.shape[1]
     gain_full = norm_gain.astype(jnp.float32)
-    raw_piece = lax.all_gather(hidden, "tp", axis=1, tiled=True).astype(jnp.float32)
+    raw_piece = jnp.concatenate(lax.all_gather(hidden, "tp"), axis=1).astype(jnp.float32)
     scaled = (raw_piece * gain_full[None, :]).astype(jnp.bfloat16)
 
     def add_product(weight):

time: 136 us -> 145 us (1.066)
  local copies, waits for them, and re-layouts: 23.9 us -> 28.8 us
  other arithmetic: 12 us -> 14.7 us
    convert_element_type x0 -> x2, other arithmetic: none -> 5.83 us  [the longest x1 3.6 us: local(): jnp.concatenate(lax.all_gather(hidden, 'tp'), axis=1).astype(jnp.float32)]
    convert_element_type x0 -> x1, local copies, waits for them, and re-layouts: none -> 3.57 us  [local(): jnp.concatenate(lax.all_gather(hidden, 'tp'), axis=1).astype(jnp.float32)]
    reduce_sum x1, other arithmetic: 1.91 us -> 0.39 us  [local(): squares = jnp.sum(raw_piece * raw_piece, axis=1)]
    unnamed x81 -> x83, local copies, waits for them, and re-layouts: 8.5 us -> 8.89 us
  transfers between devices with their start and end apart: 6 -> 6, of which waited for: 3 -> 3; matrix products, arithmetic and copies ran while one was open for 16% -> 21% of each run, Pallas kernels for 0% -> 0%
where the time goes in v1:
time: 145 us; the launch traced here: 144 us
  waiting for transfers between devices  50.4 us (35%)
  local copies, waits for them, and re-layouts  28.8 us (20%)
  matrix products  15.9 us (11%)
  between operations  14.8 us (10%)
  other arithmetic  14.7 us (10%)
  starting transfers between devices  11 us (8%)
  blocking collectives  8.71 us (6%)
    ppermute x4, waiting for transfers between devices, from_behind(): lax.ppermute(value, axis, [(source, source + steps) for source in range(i...  28.2 us
    all_gather x1, waiting for transfers between devices, local(): lax.all_gather(hidden, 'tp')  21.5 us
    unnamed x83, local copies, waits for them, and re-layouts  8.89 us
    all_gather x1, blocking collectives, local(): lax.all_gather(attended, 'tp', axis=1, tiled=True)  8.71 us
    ppermute x4, starting transfers between devices, from_behind(): lax.ppermute(value, axis, [(source, source + steps) for source in range(i...  6.63 us
    dot_general x3, matrix products, add_product(): return jnp.dot(scaled, weight, preferred_element_type=jnp.float32)  6.52 us
    all_to_all x1, starting transfers between devices, local(): lax.all_to_all(w_out, 'tp', split_axis=1, concat_axis=0, tiled=True)  4.29 us
    dot_general x3, matrix products, local_branch(): jnp.einsum('rnqhd,rnkhd->rnhqk', query_blocks, key_blocks, preferred_elem...  3.85 us
  transfers between devices with their start and end apart: 6, of which 3 were waited for; matrix products, arithmetic and copies ran while one was open for 21% of the time, Pallas kernels for 0%

profile of v1, /device:TPU:17, one launch (start us, length us, event | category | flops | bytes accessed | tf_op | source)
XLA Modules:
  0.0 144.3 jit_solution(7561649813260578083)
XLA Ops:
  7.2 0.7 all-gather.3.cloned.1.call-update
  7.9 2.3 %copy.170 = bf16[256,2048]{0,1:T(8,128)(2,1)} copy(bf16[256,2048]{1,0:T(8,128)(2,1)} %param.15) | data formatting | bytes 2097152 | tf_op args[7]
  10.2 4.3 %all-to-all-start = ((bf16[256,4,512]{0,2,1:T(8,128)(2,1)}), bf16[256,4,512]{0,2,1:T(8,128)(2,1)S(1)}, u32[]{:S(2)}, u32[]{:S(2)}) async-start(bf16[256,4,512]{0,2,1:T(8,128)(2,1)} %bitcast.69), calls=%async_computation | async-start | bytes 2097152 | tf_op jit(solution)/shard_map/all_to_all | solution.py:166
  15.0 0.7 broadcast_and_fusion.1
  15.6 0.7 broadcast_and_fusion.2
  16.3 0.8 multiply_cosine_fusion
  17.1 21.5 %all-gather.3.cloned.1.call-done = bf16[1536,512]{1,0:T(8,128)(2,1)} async-done(((bf16[384,512]{1,0:T(8,128)(2,1)}), bf16[1536,512]{1,0:T(8,128)(2,1)}) %all-gather.3.cloned.1.call-update) | async-done | bytes 1572880 | tf_op jit(solution)/shard_map/all_gather | solution.py:128
  38.6 3.6 %convert_bitcast_fusion = f32[384,4,512]{2,0,1:T(8,128)} fusion(bf16[4,384,512]{2,1,0:T(8,128)(2,1)} %bitcast.185), kind=kLoop, calls=%fused_computation.1 | loop fusion | flops 786432 | bytes 4718592 | tf_op jit(solution)/shard_map/convert_element_type | solution.py:128
  42.5 3.6 %copy.135 = f32[384,4,512]{0,2,1:T(8,128)} copy(f32[384,4,512]{2,0,1:T(8,128)} %convert_bitcast_fusion) | data formatting | bytes 6291456 | tf_op jit(solution)/shard_map/convert_element_type | solution.py:128
  46.1 2.2 %fusion.1 = bf16[384,2048]{0,1:T(8,128)(2,1)S(1)} fusion(f32[384,4,512]{0,2,1:T(8,128)} %copy.135, f32[2048]{0:T(1024)S(1)} %convert_element_type.70), kind=kLoop, calls=%fused_computation.4 | loop fusion | flops 1572864 | bytes 4726784 | tf_op jit(solution)/shard_map/convert_element_type | solution.py:129
  48.4 0.8 multiply_reduce_fusion
  49.7 3.2 %multiply_reduce_fusion.1 = (f32[384,2]{0,1:T(2,128)S(1)}, f32[384,256]{0,1:T(8,128)}) fusion(f32[384]{0:T(512)S(1)} %add_rsqrt_fusion.2, bf16[384,2048]{0,1:T(8,128)(2,1)} %copy-done.16, bf16[2048,256]{1,0:T(8,128)(2,1)} %param.10), kind=kOutput, calls=%fused_computation.70 | convolution fusion | flops 402947328 | bytes 3019264 | tf_op jit(solution)/shard_map/dot_general | solution.py:132
  52.9 1.1 copy.136
  55.1 2.5 %fusion.15 = bf16[1,384,256]{1,2,0:T(8,128)(2,1)S(1)} fusion(bf16[384,2048]{0,1:T(8,128)(2,1)} %copy-done.16, bf16[2048,256]{1,0:T(8,128)(2,1)} %param.12, f32[384]{0:T(512)S(1)} %add_rsqrt_fusion.2), kind=kOutput, calls=%fused_computation.26 | convolution fusion | flops 402849792 | bytes 2819584 | tf_op jit(solution)/shard_map/dot_general | solution.py:132
  57.6 0.8 pad_maximum_fusion.2
  58.4 0.7 collective-permute-start.2
  59.1 1.4 collective-permute-start.3
  60.6 0.7 broadcast_and_fusion
  61.2 1.3 copy.171
  62.6 1.3 collective-permute-start.1
  63.8 3.3 %collective-permute-start = (bf16[2,384,256]{1,2,0:T(8,128)(2,1)}, bf16[2,384,256]{1,2,0:T(8,128)(2,1)S(1)}, u32[]{:S(2)}, u32[]{:S(2)}) collective-permute-start(bf16[2,384,256]{1,2,0:T(8,128)(2,1)} %pad_maximum_fusion.2), channel_id=1, source_target_pairs={{0,4},{4,8},{8,12},{1,5},{5,9},{9,13},{2,6},{6,10},{10,14},{3,7},{... | collective-permute-start | bytes 1179656 | tf_op jit(solution)/shard_map/ppermute | solution.py:18
  67.1 0.7 copy.153
  67.8 0.7 copy.152
  68.6 0.7 copy.148
  69.3 0.7 copy.147
  70.2 1.1 constant_dynamic-update-slice_fusion.3
  71.2 10.8 %collective-permute-done.1 = bf16[2,384,256]{1,2,0:T(8,128)(2,1)S(1)} collective-permute-done((bf16[2,384,256]{1,2,0:T(8,128)(2,1)}, bf16[2,384,256]{1,2,0:T(8,128)(2,1)S(1)}, u32[]{:S(2)}, u32[]{:S(2)}) %collective-permute-start.1) | collective-permute-done | bytes 393248 | tf_op jit(solution)/shard_map/ppermute | solution.py:18
  82.1 17.4 %collective-permute-done = bf16[2,384,256]{1,2,0:T(8,128)(2,1)S(1)} collective-permute-done((bf16[2,384,256]{1,2,0:T(8,128)(2,1)}, bf16[2,384,256]{1,2,0:T(8,128)(2,1)S(1)}, u32[]{:S(2)}, u32[]{:S(2)}) %collective-permute-start) | collective-permute-done | bytes 393248 | tf_op jit(solution)/shard_map/ppermute | solution.py:18
  99.6 0.6 copy-done.4
  100.5 1.5 %copy.154 = bf16[1,2432,256]{2,1,0:T(8,128)(2,1)} copy(bf16[1,2432,256]{1,2,0:T(8,128)(2,1)S(1)} %get-tuple-element.2) | data formatting | bytes 2490368 | tf_op jit(solution)/shard_map/slice | solution.py:57
  102.0 2.9 %reshape.541 = bf16[152,16,2,128]{3,2,1,0:T(2,128)(2,1)S(1)} reshape(bf16[1,2432,256]{2,1,0:T(8,128)(2,1)} %copy.154) | data formatting | bytes 2490368 | tf_op jit(solution)/shard_map/reshape | solution.py:62
  104.9 2.0 %fusion.78 = (f32[16,2,24]{2,1,0:T(2,128)S(1)}, f32[16,2,24,152]{3,2,1,0:T(8,128)S(1)}) fusion(bf16[152,16,2,128]{3,2,1,0:T(2,128)(2,1)S(1)} %reshape.541, bf16[24,16,2,64]{3,0,2,1:T(8,128)(2,1)} %copy.153, bf16[24,16,2,64]{3,0,2,1:T(8,128)(2,1)} %copy.152, pred[16,24,152]{2,1,0:T(8,128)(4,1)} %broadcast_and_fusion), kind=kOutput, calls=%fused_computation.143 | convolution fusion | flops 30627072 | bytes 1970176 | tf_op jit(solution)/shard_map/rnqhd,rnkhd->rnhqk/dot_general | solution.py:87
  106.9 0.9 copy-done.6
  108.1 0.6 copy-done.22
  108.8 0.7 stack_reshape.14
  109.5 0.7 stack.54
  110.2 2.1 %maximum_maximum_fusion = (bf16[1,896,256]{1,2,0:T(8,128)(2,1)S(1)}, bf16[1,896,256]{1,2,0:T(8,128)(2,1)}) fusion(bf16[1,384,256]{1,2,0:T(8,128)(2,1)} %copy-done.8, bf16[1,384,256]{1,2,0:T(8,128)(2,1)} %bitcast.189, bf16[2,384,256]{1,2,0:T(8,128)(2,1)} %copy-done.4, bf16[2,384,256]{1,2,0:T(8,128)(2,1)} %copy-done.15), kind=kLoop, calls=%fused_computation.44 | loop fusion | flops 3670016 | bytes 2097152 | tf_op jit(solution)/shard_map/slice | solution.py:57
  112.6 1.5 %fusion.79 = (f32[4,2,96]{2,1,0:T(2,128)S(1)}, f32[4,2,96,224]{3,2,1,0:T(8,128)S(1)}) fusion(bf16[224,4,2,128]{3,2,1,0:T(2,128)(2,1)S(1)} %reshape.539, bf16[96,4,2,64]{3,0,2,1:T(8,128)(2,1)S(1)} %copy-done.19, bf16[96,4,2,64]{3,0,2,1:T(8,128)(2,1)} %copy.147, pred[4,96,224]{2,1,0:T(8,128)(4,1)S(1)} %copy-done.21), kind=kOutput, calls=%fused_computation.144 | convolution fusion | flops 44948736 | bytes 1432576 | tf_op jit(solution)/shard_map/rnqhd,rnkhd->rnhqk/dot_general | solution.py:87
  114.5 0.5 copy-done.17
  115.1 0.7 stack_reshape.13
  115.9 0.7 stack.53
  116.6 0.8 copy.166
  117.3 1.2 reshape.546
  118.6 2.1 %fusion.22 = f32[24,16,2,128]{3,0,2,1:T(8,128)S(1)} fusion(bf16[152,16,2,128]{3,2,1,0:T(2,128)(2,1)} %reshape.546, f32[16,2,24,152]{3,2,1,0:T(8,128)S(1)} %copy-done.7, f32[16,2,24]{2,1,0:T(2,128)S(1)} %get-tuple-element.26, f32[16,24,2]{1,2,0:T(2,128)} %bitcast.213), kind=kOutput, calls=%fused_computation.31 | convolution fusion | flops 30216192 | bytes 2111488 | tf_op jit(solution)/shard_map/rnhqk,rnkhd->rnqhd/dot_general | solution.py:102
  121.2 0.6 copy-done.18
  124.9 0.6 fusion.18
  126.2 8.7 %all_gather.11 = bf16[384,1024]{0,1:T(8,128)(2,1)S(1)} all-gather(bf16[384,256]{0,1:T(8,128)(2,1)S(1)} %bitcast.204), channel_id=1, replica_groups=mesh['grp'=2,'sp'=4,'tp'=4] {'tp'}, dimensions={1}, use_global_device_ids=true | all-gather | bytes 983040 | tf_op jit(solution)/shard_map/all_gather | solution.py:168
  134.9 2.6 %convolution_convert_fusion = bf16[384,512]{1,0:T(8,128)(2,1)} fusion(bf16[384,1024]{0,1:T(8,128)(2,1)S(1)} %all_gather.11, bf16[1024,512]{1,0:T(8,128)(2,1)} %bitcast.203), kind=kOutput, calls=%fused_computation.11 | convolution fusion | flops 402849792 | bytes 2228224 | tf_op jit(solution)/shard_map/dot_general | solution.py:167
  (132 shorter events, 8.3 us)
Async XLA Ops:
  7.2 41.2 %copy-start = (bf16[2048,256]{1,0:T(8,128)(2,1)S(1)}, bf16[2048,256]{1,0:T(8,128)(2,1)}, u32[]{:S(2)}) copy-start(bf16[2048,256]{1,0:T(8,128)(2,1)} %param.11) | copy-start | bytes 3145732
  7.2 31.4 %all-gather.3.cloned.1.call-start = ((), (), s32[]{:S(2)}) async-start(), calls=%async_computation.1 | async-start | bytes 1966080 | tf_op jit(solution)/shard_map/all_gather | solution.py:128
  10.2 4.3 %copy-start.32 = (bf16[2048]{0:T(1024)(128)(2,1)S(1)}, bf16[2048]{0:T(1024)(128)(2,1)}, u32[]{:S(2)}) copy-start(bf16[2048]{0:T(1024)(128)(2,1)} %param.9) | copy-start | bytes 12292
  10.2 51.1 %all-to-all-start = ((bf16[256,4,512]{0,2,1:T(8,128)(2,1)}), bf16[256,4,512]{0,2,1:T(8,128)(2,1)S(1)}, u32[]{:S(2)}, u32[]{:S(2)}) async-start(bf16[256,4,512]{0,2,1:T(8,128)(2,1)} %bitcast.69), calls=%async_computation | async-start | bytes 2097152 | tf_op jit(solution)/shard_map/all_to_all | solution.py:166
  38.6 3.6 %copy-start.1 = (bf16[1536,512]{1,0:T(8,128)(2,1)S(1)}, bf16[1536,512]{1,0:T(8,128)(2,1)}, u32[]{:S(2)}) copy-start(bf16[1536,512]{1,0:T(8,128)(2,1)} %all-gather.3.cloned.1.call-done) | copy-start | bytes 4718596
  48.4 1.2 copy-start.16
  49.7 4.4 %copy-start.33 = (f32[2,128]{1,0:T(2,128)S(1)}, f32[2,128]{1,0:T(2,128)}, u32[]{:S(2)}) copy-start(f32[2,128]{1,0:T(2,128)} %param.14) | copy-start | bytes 3076
  49.7 4.4 %copy-start.34 = (f32[2,128]{1,0:T(2,128)S(1)}, f32[2,128]{1,0:T(2,128)}, u32[]{:S(2)}) copy-start(f32[2,128]{1,0:T(2,128)} %param.13) | copy-start | bytes 3076
  54.8 13.8 %copy-start.13 = (bf16[384,2,64]{2,0,1:T(8,128)(2,1)}, bf16[384,2,64]{2,0,1:T(8,128)(2,1)S(1)}, u32[]{:S(2)}) copy-start(bf16[384,2,64]{2,0,1:T(8,128)(2,1)S(1)} %get-tuple-element.9) | copy-start | bytes 294916
  54.8 14.5 %copy-start.11 = (bf16[384,2,64]{2,0,1:T(8,128)(2,1)}, bf16[384,2,64]{2,0,1:T(8,128)(2,1)S(1)}, u32[]{:S(2)}) copy-start(bf16[384,2,64]{2,0,1:T(8,128)(2,1)S(1)} %get-tuple-element.8) | copy-start | bytes 294916
  55.1 44.5 %copy-start.2 = (bf16[384,2,128]{0,2,1:T(8,128)(2,1)}, bf16[384,2,128]{0,2,1:T(8,128)(2,1)S(1)}, u32[]{:S(2)}) copy-start(bf16[384,2,128]{0,2,1:T(8,128)(2,1)S(1)} %copy.142) | copy-start | bytes 589828
  57.6 42.0 %copy-start.8 = (bf16[1,384,256]{1,2,0:T(8,128)(2,1)}, bf16[1,384,256]{1,2,0:T(8,128)(2,1)S(1)}, u32[]{:S(2)}) copy-start(bf16[1,384,256]{1,2,0:T(8,128)(2,1)S(1)} %fusion.15) | copy-start | bytes 589828
  58.4 11.5 %collective-permute-start.2 = (bf16[2,384,256]{1,2,0:T(8,128)(2,1)}, bf16[2,384,256]{1,2,0:T(8,128)(2,1)S(1)}, u32[]{:S(2)}, u32[]{:S(2)}) collective-permute-start(bf16[2,384,256]{1,2,0:T(8,128)(2,1)} %pad_maximum_fusion.2), channel_id=1, source_target_pairs={} | collective-permute-start | bytes 1179656 | tf_op jit(solution)/shard_map/ppermute | solution.py:18
  59.1 11.0 %collective-permute-start.3 = (bf16[2,384,256]{1,2,0:T(8,128)(2,1)}, bf16[2,384,256]{1,2,0:T(8,128)(2,1)}, u32[]{:S(2)}, u32[]{:S(2)}) collective-permute-start(bf16[2,384,256]{1,2,0:T(8,128)(2,1)} %pad_maximum_fusion.2), channel_id=1, source_target_pairs={{0,12},{1,13},{2,14},{3,15},{16,28},{17,29},{18,30},{19,31}} | collective-permute-start | bytes 1179656 | tf_op jit(solution)/shard_map/ppermute | solution.py:18
  62.6 19.5 %collective-permute-start.1 = (bf16[2,384,256]{1,2,0:T(8,128)(2,1)}, bf16[2,384,256]{1,2,0:T(8,128)(2,1)S(1)}, u32[]{:S(2)}, u32[]{:S(2)}) collective-permute-start(bf16[2,384,256]{1,2,0:T(8,128)(2,1)} %pad_maximum_fusion.2), channel_id=1, source_target_pairs={{0,8},{4,12},{1,9},{5,13},{2,10},{6,14},{3,11},{7,15},{16,24},{20,... | collective-permute-start | bytes 1179656 | tf_op jit(solution)/shard_map/ppermute | solution.py:18
  63.8 35.7 %collective-permute-start = (bf16[2,384,256]{1,2,0:T(8,128)(2,1)}, bf16[2,384,256]{1,2,0:T(8,128)(2,1)S(1)}, u32[]{:S(2)}, u32[]{:S(2)}) collective-permute-start(bf16[2,384,256]{1,2,0:T(8,128)(2,1)} %pad_maximum_fusion.2), channel_id=1, source_target_pairs={{0,4},{4,8},{8,12},{1,5},{5,9},{9,13},{2,6},{6,10},{10,14},{3,7},{... | collective-permute-start | bytes 1179656 | tf_op jit(solution)/shard_map/ppermute | solution.py:18
  82.1 17.6 %copy-start.15 = (bf16[2,384,256]{1,2,0:T(8,128)(2,1)}, bf16[2,384,256]{1,2,0:T(8,128)(2,1)S(1)}, u32[]{:S(2)}) copy-start(bf16[2,384,256]{1,2,0:T(8,128)(2,1)S(1)} %collective-permute-done.1) | copy-start | bytes 1179652
  99.5 0.7 copy-start.4
  106.9 0.9 copy-start.6
  108.1 0.6 copy-start.22
  110.2 2.5 %copy-start.19 = (bf16[96,4,2,64]{3,0,2,1:T(8,128)(2,1)S(1)}, bf16[96,4,2,64]{3,0,2,1:T(8,128)(2,1)}, u32[]{:S(2)}) copy-start(bf16[96,4,2,64]{3,0,2,1:T(8,128)(2,1)} %copy.148) | copy-start | bytes 294916
  110.2 2.5 %copy-start.21 = (pred[4,96,224]{2,1,0:T(8,128)(4,1)S(1)}, pred[4,96,224]{2,1,0:T(8,128)(4,1)}, u32[]{:S(2)}) copy-start(pred[4,96,224]{2,1,0:T(8,128)(4,1)} %broadcast_and_fusion.1) | copy-start | bytes 258052
  114.1 0.9 copy-start.17
  114.1 2.5 %copy-start.25 = (f32[4,2,96]{2,1,0:T(2,128)}, f32[4,2,96]{2,1,0:T(2,128)S(1)}, u32[]{:S(2)}) copy-start(f32[4,2,96]{2,1,0:T(2,128)S(1)} %get-tuple-element.28) | copy-start | bytes 9220
  115.0 1.6 %copy-start.27 = (f32[4,2,96]{2,1,0:T(2,128)}, f32[4,2,96]{2,1,0:T(2,128)S(1)}, u32[]{:S(2)}) copy-start(f32[4,2,96]{2,1,0:T(2,128)S(1)} %fusion.28) | copy-start | bytes 9220
  117.3 1.3 copy-start.7
  118.6 2.2 %copy-start.10 = (bf16[1,896,256]{1,2,0:T(8,128)(2,1)S(1)}, bf16[1,896,256]{1,2,0:T(8,128)(2,1)}, u32[]{:S(2)}) copy-start(bf16[1,896,256]{1,2,0:T(8,128)(2,1)} %get-tuple-element.5) | copy-start | bytes 1376260
  120.7 1.1 copy-start.18
  120.7 1.1 copy-start.26
  120.7 1.1 copy-start.28
  121.8 0.9 copy-start.3
  121.8 1.1 copy-start.5
  121.8 1.1 copy-start.9
  123.0 0.9 copy-start.12
  123.0 1.0 copy-start.14
  123.0 1.1 copy-start.20
  124.8 0.7 copy-start.29
  124.9 0.7 copy-start.30
  124.9 0.7 copy-start.23
  124.9 0.7 copy-start.24
  125.6 11.9 %copy-start.31 = (f32[384,2]{0,1:T(2,128)}, f32[384,2]{0,1:T(2,128)S(1)}, u32[]{:S(2)}) copy-start(f32[384,2]{0,1:T(2,128)S(1)} %log_add_fusion) | copy-start | bytes 9220
Sparse Core Ops, SparseCore 0:
  9.5 28.9 all-gather.2
